TPU v7x, 32 devices: a whole 2x2x4 slice. The times are simulated.
32 devices in a mesh: sp: 8 (over z, y), tp: 4 (over x, core).
Axes of the slice: x: 2, y: 2, z: 4, core: 2. Of those that a mesh axis runs over, the one named last changes fastest.
Arguments:
- cotangent: bfloat16 [2048, 2048], P('sp'), may hold values from -6 to 6
- stream_in: bfloat16 [2048, 2048], P('sp'), may hold values from -6 to 6
- norm_gain: float32 [2048], replicated, may hold values from 0.1 to 1.9
- out_gate: bfloat16 [2048, 1024], P('sp', 'tp'), may hold values from -6 to 6
- in_gate: bfloat16 [2048, 1024], P('sp', 'tp'), may hold values from -6 to 6
- conv_input: bfloat16 [2048, 1024], P('sp', 'tp'), may hold values from -6 to 6
- conv_taps: float32 [3, 1024], P(None, 'tp'), may hold values from -3 to 3
- out_weight: bfloat16 [2048, 1024], P(None, 'tp'), may hold values from -0.1875 to 0.1875
- expert_gate: bfloat16 [8, 2048, 1024], P('sp', None, 'tp'), may hold values from -0.125 to 0.125
- expert_up: bfloat16 [8, 2048, 1024], P('sp', None, 'tp'), may hold values from -0.125 to 0.125
- expert_down: bfloat16 [8, 1024, 2048], P('sp', 'tp'), may hold values from -0.1875 to 0.1875
- expert_choice: int32 [2048, 2], P('sp'), may hold values from 0 to 7, all different within a row; in each aligned block of 256 rows (0 to 255, 256 to 511, ...) at most 128 rows name the same one
- route_scale: float32 [2048, 2], P('sp'), may hold values from 0.05 to 0.6
Outputs:
- grad_stream: bfloat16 [2048, 2048], P('sp', 'tp')
- grad_out_gate: bfloat16 [2048, 1024], P('sp', 'tp')
- grad_in_gate: bfloat16 [2048, 1024], P('sp', 'tp')
- grad_conv_input: bfloat16 [2048, 1024], P('sp', 'tp')
- grad_out_weight: float32 [2048, 1024], P('sp', 'tp')
- grad_expert_gate: float32 [8, 2048, 1024], P('sp', None, 'tp')
- grad_expert_up: float32 [8, 2048, 1024], P('sp', None, 'tp')
- grad_expert_down: float32 [8, 1024, 2048], P('sp', 'tp')
Inputs may be any that keep to these rules, and one draw needn't show every extreme that they name: `expert_choice`: each row names two different experts. Within the rows of one device no expert is named more than 128 times, a bound that some block reaches in some devices' rows.
All inputs are finite; a program needn't handle non-finite values.
Results may differ from a plain program's by a relative error of at most 0.01.
Values may be sent and summed in bfloat16 or wider, within the bound.
A program may use at most 128 MiB of HBM per device.

v0:
```python
import jax
import jax.numpy as jnp
from jax import lax
from jax.sharding import PartitionSpec as P

norm_eps = 1e-06


def passed_along(value, axis, steps):
    count = lax.axis_size(axis)
    first, last = (max(0, -steps), min(count, count - steps))
    return lax.ppermute(value, axis, [(source, source + steps) for source in range(first, last)])


def slot_table(choice_rows, expert_count, capacity):
    flat_ids = choice_rows.reshape(-1)
    route_count = flat_ids.shape[0]
    onehot = (flat_ids[:, None] == jnp.arange(expert_count, dtype=jnp.int32)[None, :]).astype(
        jnp.int32
    )
    earlier = jnp.cumsum(onehot, axis=0) - onehot
    position = jnp.sum(earlier * onehot, axis=1)
    slot_of_route = flat_ids * capacity + position
    route_of_slot = jnp.full((expert_count * capacity,), route_count, jnp.int32)
    route_of_slot = route_of_slot.at[slot_of_route].set(jnp.arange(route_count, dtype=jnp.int32))
    return (slot_of_route, route_of_slot)


def rows_product(left, right):
    return lax.dot_general(
        left, right, (((0,), (0,)), ((), ())), preferred_element_type=jnp.float32
    )


def cols_product(left, right):
    return lax.dot_general(
        left, right, (((1,), (1,)), ((), ())), preferred_element_type=jnp.float32
    )


def shards(
    cotangent,
    stream_in,
    norm_gain,
    out_gate,
    in_gate,
    conv_input,
    conv_taps,
    out_weight,
    expert_gate,
    expert_up,
    expert_down,
    expert_choice,
    route_scale,
):
    sp_size = lax.axis_size("sp")
    tp_size = lax.axis_size("tp")
    rows_here = stream_in.shape[0]
    model_width = stream_in.shape[1]
    column_width = model_width // tp_size
    column_start = lax.axis_index("tp") * column_width
    capacity = 4 * rows_here // sp_size
    route_count = 2 * rows_here
    stream = stream_in.astype(jnp.float32)
    inverse_rms = lax.rsqrt(jnp.mean(stream * stream, axis=-1, keepdims=True) + norm_eps)
    unit_stream = stream * inverse_rms
    normed = (unit_stream * norm_gain).astype(jnp.bfloat16)
    slot_of_route, route_of_slot = slot_table(expert_choice, sp_size, capacity)
    present = route_of_slot < route_count
    safe_route = jnp.where(present, route_of_slot, 0)
    token = safe_route // 2
    weight = jnp.where(present, route_scale.reshape(-1)[safe_route], jnp.zeros((), jnp.float32))
    scaled_send = (cotangent[token].astype(jnp.float32) * weight[:, None]).astype(jnp.bfloat16)
    rows_send = jnp.where(present[:, None], normed[token], jnp.zeros((), jnp.bfloat16))
    scaled_part = lax.dynamic_slice_in_dim(scaled_send, column_start, column_width, 1)
    rows_part = lax.dynamic_slice_in_dim(rows_send, column_start, column_width, 1)
    scaled_recv, rows_recv = (
        lax.all_to_all(scaled_part, "sp", split_axis=0, concat_axis=0, tiled=True),
        lax.all_to_all(rows_part, "sp", split_axis=0, concat_axis=0, tiled=True),
    )
    scaled_cot, expert_rows = (
        lax.all_gather(scaled_recv, "tp", axis=1, tiled=True),
        lax.all_gather(rows_recv, "tp", axis=1, tiled=True),
    )
    w_gate = expert_gate[0]
    w_up = expert_up[0]
    w_down = expert_down[0]
    gate_pre = jnp.dot(expert_rows, w_gate, preferred_element_type=jnp.float32)
    up_pre = jnp.dot(expert_rows, w_up, preferred_element_type=jnp.float32)
    sigmoid_gate = jax.nn.sigmoid(gate_pre)
    silu_gate = gate_pre * sigmoid_gate
    hidden = (silu_gate * up_pre).astype(jnp.bfloat16)
    hidden_grad = cols_product(scaled_cot, w_down)
    gate_grad = (
        hidden_grad * up_pre * sigmoid_gate * (1.0 + gate_pre * (1.0 - sigmoid_gate))
    ).astype(jnp.bfloat16)
    up_grad = (hidden_grad * silu_gate).astype(jnp.bfloat16)
    partial_grad = cols_product(gate_grad, w_gate) + cols_product(up_grad, w_up)
    slot_grad = lax.psum_scatter(
        partial_grad.astype(jnp.bfloat16), "tp", scatter_dimension=1, tiled=True
    )
    returned = lax.all_to_all(slot_grad, "sp", split_axis=0, concat_axis=0, tiled=True)
    grad_down = rows_product(hidden, scaled_cot)[None]
    grad_gate = rows_product(expert_rows, gate_grad)[None]
    grad_up = rows_product(expert_rows, up_grad)[None]
    product = in_gate.astype(jnp.float32) * conv_input.astype(jnp.float32)
    earlier = passed_along(product[-2:], "sp", 1)
    extended = jnp.concatenate([earlier, product], axis=0)
    filtered = conv_taps[0] * product + conv_taps[1] * extended[1:-1] + conv_taps[2] * extended[:-2]
    mixed_in = (out_gate.astype(jnp.float32) * filtered).astype(jnp.bfloat16)
    token_cols = returned[slot_of_route].astype(jnp.float32).reshape(rows_here, 2, column_width)
    token_cols = jnp.sum(token_cols, axis=1).astype(jnp.bfloat16)
    token_grad = lax.all_gather(token_cols, "tp", axis=1, tiled=True)
    unit_grad = token_grad.astype(jnp.float32) * norm_gain
    along = jnp.mean(unit_stream * unit_grad, axis=-1, keepdims=True)
    stream_grad = (
        cotangent.astype(jnp.float32) + inverse_rms * (unit_grad - unit_stream * along)
    ).astype(jnp.bfloat16)
    grad_stream = lax.dynamic_slice_in_dim(stream_grad, column_start, column_width, 1)
    mixed_grad = jnp.dot(stream_grad, out_weight, preferred_element_type=jnp.float32)
    grad_out_gate = (mixed_grad * filtered).astype(jnp.bfloat16)
    filtered_grad = mixed_grad * out_gate.astype(jnp.float32)
    later = passed_along(filtered_grad[:2], "sp", -1)
    extended_grad = jnp.concatenate([filtered_grad, later], axis=0)
    product_grad = (
        conv_taps[0] * filtered_grad
        + conv_taps[1] * extended_grad[1:-1]
        + conv_taps[2] * extended_grad[2:]
    )
    grad_in_gate = (product_grad * conv_input.astype(jnp.float32)).astype(jnp.bfloat16)
    grad_conv_input = (product_grad * in_gate.astype(jnp.float32)).astype(jnp.bfloat16)
    grad_out_weight = lax.psum_scatter(
        rows_product(stream_grad, mixed_in), "sp", scatter_dimension=0, tiled=True
    )
    return (
        grad_stream,
        grad_out_gate,
        grad_in_gate,
        grad_conv_input,
        grad_out_weight,
        grad_gate,
        grad_up,
        grad_down,
    )


def solution(mesh):
    placed = (
        P("sp", None),
        P("sp", None),
        P(),
        P("sp", "tp"),
        P("sp", "tp"),
        P("sp", "tp"),
        P(None, "tp"),
        P(None, "tp"),
        P("sp", None, "tp"),
        P("sp", None, "tp"),
        P("sp", "tp", None),
        P("sp", None),
        P("sp", None),
    )
    return jax.shard_map(
        shards,
        mesh=mesh,
        in_specs=placed,
        out_specs=(
            P("sp", "tp"),
            P("sp", "tp"),
            P("sp", "tp"),
            P("sp", "tp"),
            P("sp", "tp"),
            P("sp", None, "tp"),
            P("sp", None, "tp"),
            P("sp", "tp", None),
        ),
        check_vma=False,
    )
```

profile of v0, /device:TPU:0, one launch (start us, length us, event | category | flops | bytes accessed | tf_op | source)
XLA Modules:
  0.0 325.4 jit_solution(15488378320226567491)
XLA Ops:
  7.2 0.0 all-gather.6.cloned.1.call-start
  7.2 0.8 broadcast_multiply_fusion
  8.0 0.8 copy.22
  8.8 0.1 eq.29
  9.0 0.1 eq.25
  9.1 1.5 fusion.9
  10.6 0.1 copy.21
  10.8 0.1 mul.163
  10.9 1.1 reduce-window.6
  12.1 0.2 slice_reduce_fusion
  12.3 0.1 fusion.37
  12.5 2.4 scatter_custom_fusion
  14.9 1.5 fusion.3
  16.5 6.0 %gather_fusion.2 = bf16[1024,2048]{1,0:T(8,128)(2,1)} fusion(bf16[256,2048]{1,0:T(8,128)(2,1)S(1)} %fusion.3, s32[1024]{0:T(1024)S(1)} %fusion.41), kind=kCustom, calls=%fused_computation.2 | custom fusion | bytes 8392704 | tf_op jit(solution)/shard_map/gather | solution.py:74
  22.5 1.6 dynamic-slice_select_fusion
  24.1 33.0 %all_to_all.36 = bf16[8,128,512]{2,1,0:T(8,128)(2,1)} all-to-all(bf16[8,128,512]{2,1,0:T(8,128)(2,1)S(1)} %bitcast.58), channel_id=1, replica_groups=mesh['sp'=8,'tp'=4] {'sp'}, dimensions={0} | all-to-all | bytes 2097152 | tf_op jit(solution)/shard_map/all_to_all | solution.py:79
  57.1 0.0 all-gather.6.cloned.1.call-update
  57.1 0.0 all-gather.4.cloned.1.call-start
  57.2 0.1 copy.24
  57.3 0.1 reshape.89
  57.5 6.0 %gather_fusion = bf16[1024,2048]{1,0:T(8,128)(2,1)} fusion(bf16[256,2048]{1,0:T(8,128)(2,1)S(1)} %copy-done.1, s32[1024]{0:T(1024)S(1)} %fusion.41), kind=kCustom, calls=%fused_computation | custom fusion | bytes 8392704 | tf_op jit(solution)/shard_map/gather | solution.py:73
  63.5 6.9 %gather_fusion.1 = f32[1024]{0:T(1024)S(1)} fusion(f32[512]{0:T(512)S(1)} %reshape.89, s32[1024]{0:T(1024)S(1)} %get-tuple-element.12), kind=kCustom, calls=%fused_computation.1 | custom fusion | bytes 12288 | tf_op jit(solution)/shard_map/gather | solution.py:72
  70.4 1.5 multiply_convert_fusion
  71.9 29.0 %all_to_all.37 = bf16[8,128,512]{2,1,0:T(8,128)(2,1)} all-to-all(bf16[8,128,512]{2,1,0:T(8,128)(2,1)S(1)} %bitcast.55), channel_id=1, replica_groups=mesh['sp'=8,'tp'=4] {'sp'}, dimensions={0} | all-to-all | bytes 2097152 | tf_op jit(solution)/shard_map/all_to_all | solution.py:78
  100.9 0.0 all-gather.4.cloned.1.call-update
  100.9 0.0 reduce-scatter.3.cloned.1.call-start
  101.0 0.0 all-gather.6.cloned.1.call-done
  101.0 4.6 %fusion.12 = f32[1024,256]{1,0:T(8,128)} fusion(bf16[1024,2048]{1,0:T(8,128)(2,1)} %all-gather.6.cloned.1.call-done, bf16[1,2048,256]{2,1,0:T(8,128)(2,1)S(1)} %copy-done), kind=kOutput, calls=%fused_computation.26 | convolution fusion | flops 1073741824 | bytes 6291456 | tf_op jit(solution)/shard_map/dot_general | solution.py:88
  105.6 2.3 fusion.15
  107.9 26.6 %all-gather.4.cloned.1.call-done = bf16[1024,2048]{1,0:T(8,128)(2,1)} async-done(((bf16[1024,512]{1,0:T(8,128)(2,1)}), bf16[1024,2048]{1,0:T(8,128)(2,1)}) %all-gather.4.cloned.1.call-update) | async-done | bytes 4194320 | tf_op jit(solution)/shard_map/all_gather | solution.py:82
  134.5 4.6 %multiply_convert_fusion.2 = (bf16[1024,256]{1,0:T(8,128)(2,1)S(1)}, bf16[1024,256]{1,0:T(8,128)(2,1)S(1)}) fusion(f32[1024,256]{1,0:T(8,128)} %fusion.12, f32[1024,256]{1,0:T(8,128)} %fusion.15, bf16[1024,2048]{1,0:T(8,128)(2,1)} %all-gather.4.cloned.1.call-done, bf16[1,256,2048]{2,1,0:T(8,128)(2,1)} %param.23), kind=kOutput, calls=%fused_computation.34 | convolution fusion | flops 1077149696 | bytes 8388608 | tf_op jit(solution)/shard_map/dot_general | solution.py:36
  139.1 1.3 fusion.10
  140.4 3.3 %add_convert_fusion = bf16[1024,2048]{1,0:T(8,128)(2,1)} fusion(f32[1024,2048]{1,0:T(8,128)S(1)} %fusion.10, bf16[1024,256]{1,0:T(8,128)(2,1)S(1)} %get-tuple-element.14, bf16[1,2048,256]{2,1,0:T(8,128)(2,1)S(1)} %copy-done.4), kind=kOutput, calls=%fused_computation.5 | convolution fusion | flops 1077936128 | bytes 14155776 | tf_op jit(solution)/shard_map/dot_general | solution.py:36
  143.7 0.0 reduce-scatter.3.cloned.1.call-update
  143.7 44.6 %reduce-scatter.3.cloned.1.call-done = bf16[1024,512]{1,0:T(8,128)(2,1)} async-done(((bf16[1024,2048]{1,0:T(8,128)(2,1)}), bf16[1024,512]{1,0:T(8,128)(2,1)}) %reduce-scatter.3.cloned.1.call-update) | async-done | bytes 1048592 | tf_op jit(solution)/shard_map/reduce_scatter | solution.py:99
  188.3 5.6 %all-to-all-start.2 = ((bf16[8,128,512]{2,1,0:T(8,128)(2,1)}), bf16[8,128,512]{2,1,0:T(8,128)(2,1)S(1)}, u32[]{:S(2)}, u32[]{:S(2)}) async-start(bf16[8,128,512]{2,1,0:T(8,128)(2,1)} %bitcast.59), calls=%async_computation.3 | async-start | bytes 2097152 | tf_op jit(solution)/shard_map/all_to_all | solution.py:102
  193.9 0.2 all-gather.8.cloned.1.call-start
  194.2 25.4 %all-to-all-done.2 = bf16[8,128,512]{2,1,0:T(8,128)(2,1)S(1)} async-done(((bf16[8,128,512]{2,1,0:T(8,128)(2,1)}), bf16[8,128,512]{2,1,0:T(8,128)(2,1)S(1)}, u32[]{:S(2)}, u32[]{:S(2)}) %all-to-all-start.2) | async-done | bytes 1048608 | tf_op jit(solution)/shard_map/all_to_all | solution.py:102
  219.6 2.6 gather_fusion.3
  222.2 2.1 gather.18
  224.3 3.1 reduce_sum.44
  227.4 0.0 all-gather.8.cloned.1.call-update
  227.4 0.0 reduce-scatter.5.cloned.1.call-start
  227.5 0.7 copy-done.11
  228.2 0.6 slice.56
  228.8 3.8 %collective-permute-start = (f32[2,256]{1,0:T(2,128)}, f32[2,256]{1,0:T(2,128)}, u32[]{:S(2)}, u32[]{:S(2)}) collective-permute-start(f32[2,256]{1,0:T(2,128)} %slice.56), channel_id=1, source_target_pairs={{0,4},{4,8},{8,12},{12,16},{16,20},{20,24},{24,28},{1,5},{5,9},{9,... | collective-permute-start | bytes 6152 | tf_op jit(solution)/shard_map/ppermute | solution.py:12
  232.6 1.4 fusion.48
  234.0 8.3 %all-gather.8.cloned.1.call-done = bf16[256,2048]{1,0:T(8,128)(2,1)} async-done(((bf16[256,512]{1,0:T(8,128)(2,1)}), bf16[256,2048]{1,0:T(8,128)(2,1)}) %all-gather.8.cloned.1.call-update) | async-done | bytes 1048592 | tf_op jit(solution)/shard_map/all_gather | solution.py:113
  242.3 2.2 fusion.4
  244.5 2.0 fusion.8
  246.6 1.8 multiply_convert_fusion.5
  248.4 1.9 fusion.34
  250.3 0.0 reduce-scatter.5.cloned.1.call-update
  250.4 5.0 %convolution_bitcast_fusion.1 = f32[1,2048,256]{2,1,0:T(8,128)} fusion(bf16[1024,2048]{1,0:T(8,128)(2,1)} %all-gather.6.cloned.1.call-done, bf16[1024,256]{1,0:T(8,128)(2,1)S(1)} %copy-done.8), kind=kOutput, calls=%fused_computation.7 | convolution fusion | flops 1073741824 | bytes 6815744 | tf_op jit(solution)/shard_map/dot_general | solution.py:30
  255.4 2.7 convolution_bitcast_fusion.2
  258.1 0.3 copy-done.24
  258.3 0.6 copy-done.25
  259.0 2.7 convolution_bitcast_fusion
  261.6 1.3 collective-permute-start.1
  262.9 1.7 constant_dynamic-slice_fusion
  264.6 2.5 collective-permute-done.1
  267.1 0.8 fusion.28
  267.9 0.7 fusion.29
  268.6 50.3 %reduce-scatter.5.cloned.1.call-done = f32[256,256]{1,0:T(8,128)} async-done(((f32[2048,256]{1,0:T(8,128)}), f32[256,256]{1,0:T(8,128)}) %reduce-scatter.5.cloned.1.call-update) | async-done | bytes 262160 | tf_op jit(solution)/shard_map/reduce_scatter | solution.py:132
  (63 shorter events, 0.2 us)
Async XLA Ops:
  7.2 93.8 %copy-start = (bf16[1,2048,256]{2,1,0:T(8,128)(2,1)S(1)}, bf16[1,2048,256]{2,1,0:T(8,128)(2,1)}, u32[]{:S(2)}) copy-start(bf16[1,2048,256]{2,1,0:T(8,128)(2,1)} %param.21) | copy-start | bytes 3145732
  7.2 93.8 %all-gather.6.cloned.1.call-start = ((), (), s32[]{:S(2)}) async-start(), calls=%async_computation.6 | async-start | bytes 5242880 | tf_op jit(solution)/shard_map/all_gather | solution.py:83
  22.5 34.7 %copy-start.19 = (f32[256,2]{0,1:T(2,128)S(1)}, f32[256,2]{0,1:T(2,128)}, u32[]{:S(2)}) copy-start(f32[256,2]{0,1:T(2,128)} %param.25) | copy-start | bytes 6148
  22.5 35.0 %copy-start.1 = (bf16[256,2048]{1,0:T(8,128)(2,1)S(1)}, bf16[256,2048]{1,0:T(8,128)(2,1)}, u32[]{:S(2)}) copy-start(bf16[256,2048]{1,0:T(8,128)(2,1)} %param.13) | copy-start | bytes 3145732
  57.1 77.4 %all-gather.4.cloned.1.call-start = ((), (), s32[]{:S(2)}) async-start(), calls=%async_computation.5 | async-start | bytes 5242880 | tf_op jit(solution)/shard_map/all_gather | solution.py:82
  100.9 4.7 %copy-start.4 = (bf16[1,2048,256]{2,1,0:T(8,128)(2,1)S(1)}, bf16[1,2048,256]{2,1,0:T(8,128)(2,1)}, u32[]{:S(2)}) copy-start(bf16[1,2048,256]{2,1,0:T(8,128)(2,1)} %param.22) | copy-start | bytes 3145732
  100.9 87.4 %reduce-scatter.3.cloned.1.call-start = ((), (), s32[]{:S(2)}) async-start(), calls=%async_computation.7 | async-start | bytes 5242880 | tf_op jit(solution)/shard_map/reduce_scatter | solution.py:99
  101.0 4.6 %copy-start.20 = (bf16[1024,2048]{1,0:T(8,128)(2,1)S(1)}, bf16[1024,2048]{1,0:T(8,128)(2,1)}, u32[]{:S(2)}) copy-start(bf16[1024,2048]{1,0:T(8,128)(2,1)} %all-gather.6.cloned.1.call-done) | copy-start | bytes 12582916
  139.1 1.3 copy-start.5
  139.1 1.3 copy-start.7
  188.3 39.2 %copy-start.9 = (bf16[256,256]{1,0:T(8,128)(2,1)S(1)}, bf16[256,256]{1,0:T(8,128)(2,1)}, u32[]{:S(2)}) copy-start(bf16[256,256]{1,0:T(8,128)(2,1)} %param.17) | copy-start | bytes 393220
  188.3 39.2 %copy-start.10 = (bf16[256,256]{1,0:T(8,128)(2,1)S(1)}, bf16[256,256]{1,0:T(8,128)(2,1)}, u32[]{:S(2)}) copy-start(bf16[256,256]{1,0:T(8,128)(2,1)} %param.18) | copy-start | bytes 393220
  188.3 31.3 %all-to-all-start.2 = ((bf16[8,128,512]{2,1,0:T(8,128)(2,1)}), bf16[8,128,512]{2,1,0:T(8,128)(2,1)S(1)}, u32[]{:S(2)}, u32[]{:S(2)}) async-start(bf16[8,128,512]{2,1,0:T(8,128)(2,1)} %bitcast.59), calls=%async_computation.3 | async-start | bytes 2097152 | tf_op jit(solution)/shard_map/all_to_all | solution.py:102
  193.9 48.4 %copy-start.14 = (f32[2048]{0:T(1024)S(1)}, f32[2048]{0:T(1024)}, u32[]{:S(2)}) copy-start(f32[2048]{0:T(1024)} %param.15) | copy-start | bytes 24580
  193.9 48.4 %all-gather.8.cloned.1.call-start = ((), (), s32[]{:S(2)}) async-start(), calls=%async_computation.8 | async-start | bytes 1310720 | tf_op jit(solution)/shard_map/all_gather | solution.py:113
  222.2 22.3 %copy-start.2 = (bf16[256,2048]{1,0:T(8,128)(2,1)S(1)}, bf16[256,2048]{1,0:T(8,128)(2,1)}, u32[]{:S(2)}) copy-start(bf16[256,2048]{1,0:T(8,128)(2,1)} %param.14) | copy-start | bytes 3145732
  224.3 22.2 %copy-start.13 = (bf16[256,256]{1,0:T(8,128)(2,1)S(1)}, bf16[256,256]{1,0:T(8,128)(2,1)}, u32[]{:S(2)}) copy-start(bf16[256,256]{1,0:T(8,128)(2,1)} %param.16) | copy-start | bytes 393220
  227.4 91.5 %reduce-scatter.5.cloned.1.call-start = ((), (), s32[]{:S(2)}) async-start(), calls=%async_computation.9 | async-start | bytes 2359296 | tf_op jit(solution)/shard_map/reduce_scatter | solution.py:132
  227.5 0.7 copy-start.11
  228.8 17.7 %collective-permute-start = (f32[2,256]{1,0:T(2,128)}, f32[2,256]{1,0:T(2,128)}, u32[]{:S(2)}, u32[]{:S(2)}) collective-permute-start(f32[2,256]{1,0:T(2,128)} %slice.56), channel_id=1, source_target_pairs={{0,4},{4,8},{8,12},{12,16},{16,20},{20,24},{24,28},{1,5},{5,9},{9,... | collective-permute-start | bytes 6152 | tf_op jit(solution)/shard_map/ppermute | solution.py:12
  242.3 4.3 %copy-start.12 = (f32[256,256]{1,0:T(8,128)S(1)}, f32[256,256]{1,0:T(8,128)}, u32[]{:S(2)}) copy-start(f32[256,256]{1,0:T(8,128)} %copy-done.11) | copy-start | bytes 786436
  242.3 4.3 %copy-start.15 = (f32[1,256]{1,0:T(1,128)S(1)}, f32[1,256]{1,0:T(1,128)}, u32[]{:S(2)}) copy-start(f32[1,256]{1,0:T(1,128)} %get-tuple-element.18) | copy-start | bytes 3076
  242.3 4.3 %copy-start.17 = (f32[1,256]{1,0:T(1,128)S(1)}, f32[1,256]{1,0:T(1,128)}, u32[]{:S(2)}) copy-start(f32[1,256]{1,0:T(1,128)} %get-tuple-element.19) | copy-start | bytes 3076
  242.3 4.3 %copy-start.23 = (bf16[2048,256]{1,0:T(8,128)(2,1)S(1)}, bf16[2048,256]{1,0:T(8,128)(2,1)}, u32[]{:S(2)}) copy-start(bf16[2048,256]{1,0:T(8,128)(2,1)} %param.20) | copy-start | bytes 3145732
  246.5 1.9 copy-start.3
  246.6 3.8 %copy-start.8 = (bf16[1024,256]{1,0:T(8,128)(2,1)S(1)}, bf16[1024,256]{1,0:T(8,128)(2,1)}, u32[]{:S(2)}) copy-start(bf16[1024,256]{1,0:T(8,128)(2,1)} %copy-done.7) | copy-start | bytes 1572868
  250.4 5.0 %copy-start.6 = (bf16[1024,256]{1,0:T(8,128)(2,1)S(1)}, bf16[1024,256]{1,0:T(8,128)(2,1)}, u32[]{:S(2)}) copy-start(bf16[1024,256]{1,0:T(8,128)(2,1)} %copy-done.5) | copy-start | bytes 1572868
  250.4 5.0 %copy-start.21 = (bf16[1024,2048]{1,0:T(8,128)(2,1)S(1)}, bf16[1024,2048]{1,0:T(8,128)(2,1)}, u32[]{:S(2)}) copy-start(bf16[1024,2048]{1,0:T(8,128)(2,1)} %all-gather.6.cloned.1.call-done) | copy-start | bytes 12582916
  255.4 2.7 copy-start.22
  255.4 3.0 copy-start.24
  255.4 3.6 %copy-start.25 = (f32[1024,256]{1,0:T(8,128)S(1)}, f32[1024,256]{1,0:T(8,128)}, u32[]{:S(2)}) copy-start(f32[1024,256]{1,0:T(8,128)} %fusion.15) | copy-start | bytes 3145732
  259.0 8.1 %copy-start.16 = (f32[1,256]{1,0:T(1,128)S(1)}, f32[1,256]{1,0:T(1,128)}, u32[]{:S(2)}) copy-start(f32[1,256]{1,0:T(1,128)} %get-tuple-element.18) | copy-start | bytes 3076
  259.0 8.1 %copy-start.18 = (f32[1,256]{1,0:T(1,128)S(1)}, f32[1,256]{1,0:T(1,128)}, u32[]{:S(2)}) copy-start(f32[1,256]{1,0:T(1,128)} %get-tuple-element.19) | copy-start | bytes 3076
  261.6 5.5 %collective-permute-start.1 = (f32[2,256]{1,0:T(2,128)S(1)}, f32[2,256]{1,0:T(2,128)S(1)}, u32[]{:S(2)}, u32[]{:S(2)}) collective-permute-start(f32[2,256]{1,0:T(2,128)S(1)} %slice.59), channel_id=1, source_target_pairs={{4,0},{8,4},{12,8},{16,12},{20,16},{24,20},{28,24},{5,1},{9,5},{13... | collective-permute-start | bytes 6152 | tf_op jit(solution)/shard_map/ppermute | solution.py:12
Sparse Core Ops, SparseCore 0:
  57.2 33.4 all-gather.5
  101.0 33.4 all-gather.3
  143.8 44.3 reduce-scatter.2
  227.5 14.7 all-gather.7
  250.5 68.3 reduce-scatter.4
where the time goes:
time: 326 us; the launch traced here: 325 us
  waiting for transfers between devices  158 us (48%)
  blocking collectives  61.9 us (19%)
  local copies, waits for them, and re-layouts  33.3 us (10%)
  matrix products  30.1 us (9%)
  other arithmetic  17 us (5%)
  between operations  14.2 us (4%)
  starting transfers between devices  11.1 us (3%)
    reduce_scatter x1, waiting for transfers between devices, shards(): lax.psum_scatter(rows_product(stream_grad, mixed_in), 'sp', scatter_dimen...  50.3 us
    reduce_scatter x1, waiting for transfers between devices, shards(): lax.psum_scatter(partial_grad.astype(jnp.bfloat16), 'tp', scatter_dimensi...  44.6 us
    all_to_all x1, blocking collectives, shards(): lax.all_to_all(rows_part, 'sp', split_axis=0, concat_axis=0, tiled=True)  33 us
    all_to_all x1, blocking collectives, shards(): lax.all_to_all(scaled_part, 'sp', split_axis=0, concat_axis=0, tiled=True)  29 us
    all_gather x1, waiting for transfers between devices, shards(): lax.all_gather(scaled_recv, 'tp', axis=1, tiled=True)  26.6 us
    all_to_all x1, waiting for transfers between devices, shards(): lax.all_to_all(slot_grad, 'sp', split_axis=0, concat_axis=0, tiled=True)  25.4 us
    dot_general x4, matrix products, rows_product(): lax.dot_general(left, right, (((0,), (0,)), ((), ())), preferred_element_...  12.2 us
    dot_general x3, matrix products, cols_product(): lax.dot_general(left, right, (((1,), (1,)), ((), ())), preferred_element_...  9.15 us
  transfers between devices with their start and end apart: 8, of which 6 were waited for; matrix products, arithmetic and copies ran while one was open for 13% of the time, Pallas kernels for 0%

commit v1 on v0

v1 whole, which is shorter than its diff:
```python
import functools

import jax
import jax.numpy as jnp
from jax import lax
from jax.experimental import pallas as pl
from jax.experimental.pallas import tpu as pltpu
from jax.sharding import PartitionSpec as P

norm_eps = 1e-06


def passed_along(value, axis, steps):
    count = lax.axis_size(axis)
    first, last = (max(0, -steps), min(count, count - steps))
    return lax.ppermute(value, axis, [(source, source + steps) for source in range(first, last)])


def slot_masks(choice_rows, expert_count, capacity):
    rows = choice_rows.shape[0]
    onehot = choice_rows[:, :, None] == jnp.arange(expert_count, dtype=jnp.int32)
    member = jnp.any(onehot, axis=1).astype(jnp.bfloat16)
    at = jnp.arange(rows, dtype=jnp.int32)
    before = (at[:, None] > at[None, :]).astype(jnp.bfloat16)
    earlier = jnp.dot(before, member, preferred_element_type=jnp.float32).astype(jnp.int32)
    position = jnp.sum(jnp.where(onehot, earlier[:, None, :], 0), axis=-1)
    slot = choice_rows * capacity + position
    slots = jnp.arange(expert_count * capacity, dtype=jnp.int32)[:, None]
    return (slots == slot[:, 0][None, :], slots == slot[:, 1][None, :])


def rows_product(left, right):
    return lax.dot_general(
        left, right, (((0,), (0,)), ((), ())), preferred_element_type=jnp.float32
    )


def cols_product(left, right):
    return lax.dot_general(
        left, right, (((1,), (1,)), ((), ())), preferred_element_type=jnp.float32
    )


MESH = pl.DeviceIdType.MESH


def remote(source, target, send_sem, recv_sem, device):
    return pltpu.make_async_remote_copy(
        src_ref=source,
        dst_ref=target,
        send_sem=send_sem,
        recv_sem=recv_sem,
        device_id=device,
        device_id_type=MESH,
    )


def columns(index, width):
    return pl.ds(pl.multiple_of(index * width, width), width)


def tp_places():
    tp, count = lax.axis_index("tp"), lax.axis_size("tp")
    cross = lax.rem(tp + count // 2, count)
    partner = tp + 1 - 2 * lax.rem(tp, 2)
    return (tp, cross, partner, lax.rem(partner + count // 2, count))


def greet(exchange, cross, partner):
    barrier = pltpu.get_barrier_semaphore()
    waits = 2
    for peer in (cross, partner):
        pl.semaphore_signal(barrier, inc=1, device_id={"tp": peer}, device_id_type=MESH)
    if exchange:
        me, n = lax.axis_index("sp"), lax.axis_size("sp")
        waits = waits + n - 1

        def greet_one(k, carry):
            peer = lax.rem(me + k, n)
            pl.semaphore_signal(barrier, inc=1, device_id={"sp": peer}, device_id_type=MESH)
            return carry

        lax.fori_loop(1, n, greet_one, 0)
    pl.semaphore_wait(barrier, waits)


def gather_kernel(n, exchange, count, *refs):
    ins, outs = refs[:count], refs[count : 2 * count]
    local, send, recv_a, recv_b, recv_near = refs[2 * count :]
    rows, width = ins[0].shape
    depth = rows // n
    tp, cross, partner, _ = tp_places()
    me = lax.axis_index("sp")
    greet(exchange, cross, partner)

    def block_of(a, block, column):
        return outs[a].at[pl.ds(pl.multiple_of(block * depth, depth), depth), columns(column, width)]

    def source(k):
        return lax.rem(me - k + n, n) if exchange else k

    def sent(a, k):
        peer = lax.rem(me + k, n)
        return remote(
            ins[a].at[pl.ds(pl.multiple_of(peer * depth, depth), depth), :],
            block_of(a, me, tp),
            send.at[0, a],
            recv_a.at[a, k],
            {"sp": peer},
        )

    def send_all(k, carry):
        for a in range(count):
            sent(a, k).start()
        return carry

    def across(a, k):
        block = block_of(a, source(k), tp)
        return remote(block, block, send.at[1, a], recv_b.at[a, k], {"tp": cross})

    def relay(k):
        for a in range(count):
            if exchange and not isinstance(k, int):
                sent(a, k).wait_recv()
            block = block_of(a, source(k), tp)
            across(a, k).start()
            remote(block, block, send.at[2, a], recv_near.at[0, a], {"tp": partner}).start()

    def forward(k):
        for a in range(count):
            across(a, k).wait_recv()
            block = block_of(a, source(k), cross)
            remote(block, block, send.at[3, a], recv_near.at[1, a], {"tp": partner}).start()

    if exchange:
        lax.fori_loop(1, n, send_all, 0)
    for a in range(count):
        if exchange:
            own = pltpu.make_async_copy(
                ins[a].at[pl.ds(pl.multiple_of(me * depth, depth), depth), :],
                block_of(a, me, tp),
                local.at[a],
            )
        else:
            own = pltpu.make_async_copy(ins[a], outs[a].at[:, columns(tp, width)], local.at[a])
        own.start()
        own.wait()
    relay(0)

    def step(k, carry):
        relay(k)
        forward(k - 1)
        return carry

    lax.fori_loop(1, n, step, 0)
    forward(n - 1)
    for a in range(count):
        whole = outs[a].at[:, columns(tp, width)]
        for kind in (0, 1):
            remote(whole, whole, send.at[2, a], recv_near.at[kind, a], {"tp": partner}).wait_recv()
        for kind in (1, 2, 3):
            remote(whole, whole, send.at[kind, a], recv_near.at[0, a], {"tp": partner}).wait_send()
        if exchange:
            rest = ins[a].at[pl.ds(0, (n - 1) * depth), :]
            remote(rest, rest, send.at[0, a], recv_near.at[0, a], {"tp": partner}).wait_send()


def gathered(parts, n, exchange, collective_id):
    count = len(parts)
    rows, width = parts[0].shape
    wide = jax.ShapeDtypeStruct((rows, width * lax.axis_size("tp")), parts[0].dtype)
    return pl.pallas_call(
        functools.partial(gather_kernel, n, exchange, count),
        out_shape=[wide] * count,
        in_specs=[pl.BlockSpec(memory_space=pl.ANY)] * count,
        out_specs=[pl.BlockSpec(memory_space=pl.ANY)] * count,
        scratch_shapes=[
            pltpu.SemaphoreType.DMA((count,)),
            pltpu.SemaphoreType.DMA((4, count)),
            pltpu.SemaphoreType.DMA((count, n)),
            pltpu.SemaphoreType.DMA((count, n)),
            pltpu.SemaphoreType.DMA((2, count)),
        ],
        compiler_params=pltpu.CompilerParams(collective_id=collective_id, has_side_effects=True),
    )(*parts)


def return_kernel(
    n,
    partial,
    out,
    near,
    far_out,
    far_in,
    total,
    local,
    send_near,
    recv_near,
    send_far,
    recv_far,
    send_out,
    recv_out,
):
    width = out.shape[2]
    tp, cross, partner, diagonal = tp_places()
    me = lax.axis_index("sp")
    greet(True, cross, partner)

    def target(k):
        return lax.rem(me + k + 1, n)

    def part(k, column):
        return partial[target(k), :, columns(column, width)].astype(jnp.float32)

    def handed(j, k):
        return remote(
            partial.at[target(k), :, columns((partner, diagonal)[j], width)],
            near.at[j, k],
            send_near.at[j],
            recv_near.at[j, k],
            {"tp": partner},
        )

    def across(k):
        return remote(far_out.at[k], far_in.at[k], send_far, recv_far.at[k], {"tp": cross})

    def hand(k, carry):
        handed(1, k).start()
        handed(0, k).start()
        return carry

    def pair(k, carry):
        handed(1, k).wait_recv()
        far_out[k] = (part(k, cross) + near[1, k].astype(jnp.float32)).astype(far_out.dtype)
        across(k).start()
        return carry

    def finish(k):
        handed(0, k).wait_recv()
        across(k).wait_recv()
        total[k] = (
            part(k, tp) + near[0, k].astype(jnp.float32) + far_in[k].astype(jnp.float32)
        ).astype(total.dtype)

    def finish_remote(k, carry):
        finish(k)
        remote(total.at[k], out.at[me], send_out, recv_out, {"sp": target(k)}).start()
        return carry

    lax.fori_loop(0, n, hand, 0)
    lax.fori_loop(0, n, pair, 0)
    lax.fori_loop(0, n - 1, finish_remote, 0)
    finish(n - 1)
    own = pltpu.make_async_copy(total.at[n - 1], out.at[me], local)
    own.start()
    own.wait()
    rest, rest_out = total.at[pl.ds(0, n - 1)], out.at[pl.ds(0, n - 1)]
    remote(rest, rest_out, send_out, recv_out, {"tp": partner}).wait()
    remote(far_out, far_in, send_far, recv_out, {"tp": cross}).wait_send()
    for j in (0, 1):
        remote(far_out, near.at[j], send_near.at[j], recv_out, {"tp": partner}).wait_send()


def returned_slots(partial, n, collective_id):
    rows, wide = partial.shape
    width, depth = wide // lax.axis_size("tp"), rows // n
    kind = partial.dtype
    return pl.pallas_call(
        functools.partial(return_kernel, n),
        out_shape=jax.ShapeDtypeStruct((n, depth, width), kind),
        in_specs=[pl.BlockSpec(memory_space=pltpu.VMEM)],
        out_specs=pl.BlockSpec(memory_space=pl.ANY),
        scratch_shapes=[
            pltpu.VMEM((2, n, depth, width), kind),
            pltpu.VMEM((n, depth, width), kind),
            pltpu.VMEM((n, depth, width), kind),
            pltpu.VMEM((n, depth, width), kind),
            pltpu.SemaphoreType.DMA,
            pltpu.SemaphoreType.DMA((2,)),
            pltpu.SemaphoreType.DMA((2, n)),
            pltpu.SemaphoreType.DMA,
            pltpu.SemaphoreType.DMA((n,)),
            pltpu.SemaphoreType.DMA,
            pltpu.SemaphoreType.DMA,
        ],
        compiler_params=pltpu.CompilerParams(
            collective_id=collective_id, has_side_effects=True, vmem_limit_bytes=32 * 1024 * 1024
        ),
    )(partial.reshape(n, depth, wide)).reshape(rows, width)


def shards(
    cotangent,
    stream_in,
    norm_gain,
    out_gate,
    in_gate,
    conv_input,
    conv_taps,
    out_weight,
    expert_gate,
    expert_up,
    expert_down,
    expert_choice,
    route_scale,
):
    sp_size = lax.axis_size("sp")
    tp_size = lax.axis_size("tp")
    rows_here = stream_in.shape[0]
    model_width = stream_in.shape[1]
    column_width = model_width // tp_size
    column_start = lax.axis_index("tp") * column_width
    capacity = 4 * rows_here // sp_size
    stream = stream_in.astype(jnp.float32)
    inverse_rms = lax.rsqrt(jnp.mean(stream * stream, axis=-1, keepdims=True) + norm_eps)
    unit_stream = stream * inverse_rms
    normed = (unit_stream * norm_gain).astype(jnp.bfloat16)
    first, second = slot_masks(expert_choice, sp_size, capacity)
    placing = (first | second).astype(jnp.bfloat16)
    weight = jnp.sum(
        jnp.where(first, route_scale[:, 0][None, :], 0.0)
        + jnp.where(second, route_scale[:, 1][None, :], 0.0),
        axis=1,
    )
    cot_cols = lax.dynamic_slice_in_dim(cotangent, column_start, column_width, 1)
    normed_cols = lax.dynamic_slice_in_dim(normed, column_start, column_width, 1)
    scaled_part = (
        jnp.dot(placing, cot_cols, preferred_element_type=jnp.float32) * weight[:, None]
    ).astype(jnp.bfloat16)
    rows_part = jnp.dot(placing, normed_cols, preferred_element_type=jnp.float32).astype(
        jnp.bfloat16
    )
    expert_rows, scaled_cot = gathered((rows_part, scaled_part), sp_size, True, 1)
    w_gate = expert_gate[0]
    w_up = expert_up[0]
    w_down = expert_down[0]
    gate_pre = jnp.dot(expert_rows, w_gate, preferred_element_type=jnp.float32)
    up_pre = jnp.dot(expert_rows, w_up, preferred_element_type=jnp.float32)
    sigmoid_gate = jax.nn.sigmoid(gate_pre)
    silu_gate = gate_pre * sigmoid_gate
    hidden = (silu_gate * up_pre).astype(jnp.bfloat16)
    hidden_grad = cols_product(scaled_cot, w_down)
    gate_grad = (
        hidden_grad * up_pre * sigmoid_gate * (1.0 + gate_pre * (1.0 - sigmoid_gate))
    ).astype(jnp.bfloat16)
    up_grad = (hidden_grad * silu_gate).astype(jnp.bfloat16)
    partial_grad = cols_product(gate_grad, w_gate) + cols_product(up_grad, w_up)
    returned = returned_slots(partial_grad.astype(jnp.bfloat16), sp_size, 2)
    grad_down = rows_product(hidden, scaled_cot)[None]
    grad_gate = rows_product(expert_rows, gate_grad)[None]
    grad_up = rows_product(expert_rows, up_grad)[None]
    product = in_gate.astype(jnp.float32) * conv_input.astype(jnp.float32)
    earlier = passed_along(product[-2:], "sp", 1)
    extended = jnp.concatenate([earlier, product], axis=0)
    filtered = conv_taps[0] * product + conv_taps[1] * extended[1:-1] + conv_taps[2] * extended[:-2]
    mixed_in = (out_gate.astype(jnp.float32) * filtered).astype(jnp.bfloat16)
    token_cols = rows_product(placing, returned).astype(jnp.bfloat16)
    pieces = max(1, rows_here // 64)
    (token_grad,) = gathered((token_cols,), pieces, False, 3)
    unit_grad = token_grad.astype(jnp.float32) * norm_gain
    along = jnp.mean(unit_stream * unit_grad, axis=-1, keepdims=True)
    stream_grad = (
        cotangent.astype(jnp.float32) + inverse_rms * (unit_grad - unit_stream * along)
    ).astype(jnp.bfloat16)
    grad_stream = lax.dynamic_slice_in_dim(stream_grad, column_start, column_width, 1)
    mixed_grad = jnp.dot(stream_grad, out_weight, preferred_element_type=jnp.float32)
    grad_out_gate = (mixed_grad * filtered).astype(jnp.bfloat16)
    filtered_grad = mixed_grad * out_gate.astype(jnp.float32)
    later = passed_along(filtered_grad[:2], "sp", -1)
    extended_grad = jnp.concatenate([filtered_grad, later], axis=0)
    product_grad = (
        conv_taps[0] * filtered_grad
        + conv_taps[1] * extended_grad[1:-1]
        + conv_taps[2] * extended_grad[2:]
    )
    grad_in_gate = (product_grad * conv_input.astype(jnp.float32)).astype(jnp.bfloat16)
    grad_conv_input = (product_grad * in_gate.astype(jnp.float32)).astype(jnp.bfloat16)
    shares = rows_product(stream_grad, mixed_in).astype(jnp.bfloat16)
    shares = shares.reshape(sp_size, model_width // sp_size, -1)
    shares = lax.all_to_all(shares, "sp", split_axis=0, concat_axis=0)
    grad_out_weight = jnp.sum(shares.astype(jnp.float32), axis=0)
    return (
        grad_stream,
        grad_out_gate,
        grad_in_gate,
        grad_conv_input,
        grad_out_weight,
        grad_gate,
        grad_up,
        grad_down,
    )


def solution(mesh):
    placed = (
        P("sp", None),
        P("sp", None),
        P(),
        P("sp", "tp"),
        P("sp", "tp"),
        P("sp", "tp"),
        P(None, "tp"),
        P(None, "tp"),
        P("sp", None, "tp"),
        P("sp", None, "tp"),
        P("sp", "tp", None),
        P("sp", None),
        P("sp", None),
    )
    return jax.shard_map(
        shards,
        mesh=mesh,
        in_specs=placed,
        out_specs=(
            P("sp", "tp"),
            P("sp", "tp"),
            P("sp", "tp"),
            P("sp", "tp"),
            P("sp", "tp"),
            P("sp", None, "tp"),
            P("sp", None, "tp"),
            P("sp", "tp", None),
        ),
        check_vma=False,
    )
```

time: 326 us -> 198 us (0.61)
  waiting for transfers between devices: 158 us -> 11.5 us
  Pallas kernels: 0 us -> 128 us
  blocking collectives: 61.9 us -> 0 us
  local copies, waits for them, and re-layouts: 33.3 us -> 5.07 us
  between operations: 14.2 us -> 0.98 us
  other arithmetic: 17 us -> 11.6 us
    pallas_call x0 -> x3, Pallas kernels: none -> 128 us  [the longest x2 83.5 us: gathered(): pl.pallas_call(functools.partial(gather_kernel, n, exchange, count), out_...]
    reduce_scatter x2 -> x0, waiting for transfers between devices: 94.9 us -> none  [the longest x1 50.3 us: shards(): lax.psum_scatter(rows_product(stream_grad, mixed_in), 'sp', scatter_dimen...]
    all_to_all x2 -> x0, blocking collectives: 61.9 us -> none  [the longest x1 33 us: shards(): lax.all_to_all(rows_part, 'sp', split_axis=0, concat_axis=0, tiled=True)]
    all_gather x3 -> x0, waiting for transfers between devices: 34.9 us -> none  [the longest x1 26.6 us: shards(): lax.all_gather(scaled_recv, 'tp', axis=1, tiled=True)]
    gather x5 -> x0, local copies, waits for them, and re-layouts: 23.6 us -> none  [the longest x1 6.86 us: shards(): route_scale.reshape(-1)[safe_route]]
    all_to_all x1, waiting for transfers between devices: 25.4 us -> 8.04 us  [shards(): shares = lax.all_to_all(shares, 'sp', split_axis=0, concat_axis=0)]
    dot_general x3, matrix products: 9.15 us -> 4.16 us  [cols_product(): lax.dot_general(left, right, (((1,), (1,)), ((), ())), preferred_element_...]
    dot_general x0 -> x3, matrix products: none -> 4.99 us  [the longest x1 2.46 us: shards(): jnp.dot(placing, normed_cols, preferred_element_type=jnp.float32)]
  transfers between devices with their start and end apart: 8 -> 3, of which waited for: 6 -> 2; matrix products, arithmetic and copies ran while one was open for 13% -> 19% of each run, Pallas kernels for 0% -> 65%
where the time goes in v1:
time: 198 us; the launch traced here: 197 us
  Pallas kernels  128 us (65%)
  matrix products  28.3 us (14%)
  starting transfers between devices  12.1 us (6%)
  other arithmetic  11.6 us (6%)
  waiting for transfers between devices  11.5 us (6%)
  local copies, waits for them, and re-layouts  5.07 us (3%)
    pallas_call x2, Pallas kernels, gathered(): pl.pallas_call(functools.partial(gather_kernel, n, exchange, count), out_...  83.5 us
    pallas_call x1, Pallas kernels, returned_slots(): pl.pallas_call(functools.partial(return_kernel, n), out_shape=jax.ShapeDt...  44.3 us
    dot_general x5, matrix products, rows_product(): lax.dot_general(left, right, (((0,), (0,)), ((), ())), preferred_element_...  13.1 us
    all_to_all x1, waiting for transfers between devices, shards(): shares = lax.all_to_all(shares, 'sp', split_axis=0, concat_axis=0)  8.04 us
    ppermute x2, starting transfers between devices, passed_along(): lax.ppermute(value, axis, [(source, source + steps) for source in range(f...  6.18 us
    all_to_all x1, starting transfers between devices, shards(): shares = lax.all_to_all(shares, 'sp', split_axis=0, concat_axis=0)  5.96 us
    dot_general x3, matrix products, cols_product(): lax.dot_general(left, right, (((1,), (1,)), ((), ())), preferred_element_...  4.16 us
  transfers between devices with their start and end apart: 3, of which 2 were waited for; matrix products, arithmetic and copies ran while one was open for 19% of the time, Pallas kernels for 65%

profile of v1, /device:TPU:0, one launch (start us, length us, event | category | flops | bytes accessed | tf_op | source)
XLA Modules:
  0.0 197.5 jit_solution(9433611472207690370)
XLA Ops:
  0.6 0.0 copy-start
  0.6 0.0 copy-start.1
  0.7 1.1 convert_multiply_fusion.6
  1.8 4.9 %collective-permute-start = (f32[2,256]{1,0:T(2,128)S(1)}, f32[2,256]{1,0:T(2,128)S(1)}, u32[]{:S(2)}, u32[]{:S(2)}) collective-permute-start(f32[2,256]{1,0:T(2,128)S(1)} %slice.57), channel_id=1, source_target_pairs={{0,4},{4,8},{8,12},{12,16},{16,20},{20,24},{24,28},{1,5},{5,9},{9,... | collective-permute-start | bytes 6152 | tf_op jit(solution)/shard_map/ppermute | solution.py:16
  6.7 0.0 copy-start.12
  6.7 1.5 fusion
  8.3 0.7 fusion.40
  9.0 0.8 fusion.47
  9.7 0.2 convolution_convert_fusion.3
  9.9 0.7 select_reduce_fusion
  10.6 0.7 multiply_add_fusion
  11.3 1.5 convert_multiply_fusion
  12.8 0.0 copy-done.12
  12.8 0.1 dynamic-slice
  12.9 0.3 add_reduce_fusion
  13.2 2.4 %multiply_convert_fusion.refs_1_ = bf16[1024,512]{1,0:T(8,128)(2,1)} fusion(f32[1024]{0:T(1024)S(1)} %add_reduce_fusion, s32[256]{0:T(256)S(1)} %bitcast.60, s32[256]{0:T(256)S(1)} %bitcast.56, bf16[256,2048]{1,0:T(8,128)(2,1)} %param.13, s32[]{:T(128)S(6)} %select_n.17), kind=kOutput, calls=%fused_computation.12 | convolution fusion | flops 270270464 | bytes 1316868 | tf_op jit(solution)/shard_map/dot_general | solution.py:328
  15.6 2.5 %convolution_convert_fusion.1.refs_0_ = bf16[1024,512]{1,0:T(8,128)(2,1)} fusion(s32[256]{0:T(256)S(1)} %bitcast.61, s32[256]{0:T(256)S(1)} %bitcast.57, f32[256,2048]{1,0:T(8,128)} %convert_multiply_fusion, s32[]{:T(128)S(6)} %select_n.17, f32[512]{0:T(512)S(1)} %dynamic-slice), kind=kOutput, calls=%fused_computation.13 | convolution fusion | flops 270008320 | bytes 1576964 | tf_op jit(solution)/shard_map/dot_general | solution.py:330
  18.0 63.4 %shard_map.188 = (bf16[1024,2048]{1,0:T(8,128)(2,1)}, bf16[1024,2048]{1,0:T(8,128)(2,1)}) custom-call(bf16[1024,512]{1,0:T(8,128)(2,1)} %convolution_convert_fusion.1.refs_0_, bf16[1024,512]{1,0:T(8,128)(2,1)} %multiply_convert_fusion.refs_1_), custom_call_target="tpu_custom_call" | custom-call | tf_op jit(solution)/shard_map/pallas_call | solution.py:172
  81.4 0.0 copy-start.3
  81.5 3.6 %fusion.3 = f32[1024,256]{1,0:T(8,128)S(1)} fusion(bf16[1024,2048]{1,0:T(8,128)(2,1)} %get-tuple-element.11, bf16[1,2048,256]{2,1,0:T(8,128)(2,1)S(1)} %copy-done), kind=kOutput, calls=%fused_computation.18 | convolution fusion | flops 1073741824 | bytes 6291456 | tf_op jit(solution)/shard_map/dot_general | solution.py:337
  85.1 0.1 copy-done.16
  85.2 1.3 fusion.6
  86.5 0.0 copy-start.22
  86.5 0.0 copy-done.20
  86.5 1.7 copy-done.14
  88.2 0.3 copy-done.18
  88.5 1.6 multiply_convert_fusion.2
  90.1 0.0 copy-start.5
  90.1 1.3 fusion.1
  91.4 0.0 copy-done.5
  91.4 0.0 copy-done.7
  91.4 1.3 add_convert_fusion
  92.7 44.3 %shard_map.189 = bf16[8,128,512]{2,1,0:T(8,128)(2,1)S(1)} custom-call(bf16[8,128,2048]{2,1,0:T(8,128)(2,1)S(1)} %bitcast.46), custom_call_target="tpu_custom_call" | custom-call | tf_op jit(solution)/shard_map/pallas_call | solution.py:268
  137.0 1.2 convolution_convert_fusion.2.refs_0_
  138.2 20.2 %shard_map.190 = bf16[256,2048]{1,0:T(8,128)(2,1)} custom-call(bf16[256,512]{1,0:T(8,128)(2,1)} %convolution_convert_fusion.2.refs_0_), custom_call_target="tpu_custom_call" | custom-call | tf_op jit(solution)/shard_map/pallas_call | solution.py:172
  158.4 0.0 copy-start.4
  158.4 1.9 multiply_reduce_fusion
  160.4 0.0 copy-start.13
  160.4 0.0 copy-start.11
  160.4 0.0 copy-start.19
  160.4 0.8 add_convert_fusion.1
  161.2 0.0 copy-done.13
  161.2 0.0 collective-permute-done
  161.2 0.0 copy-done.11
  161.3 0.4 copy-done.19
  161.7 1.2 multiply_convert_fusion.5
  162.9 1.5 convolution_convert_fusion
  164.4 6.0 %all-to-all-start = ((bf16[8,256,256]{2,1,0:T(8,128)(2,1)}), bf16[8,256,256]{2,1,0:T(8,128)(2,1)S(1)}, u32[]{:S(2)}, u32[]{:S(2)}) async-start(bf16[8,256,256]{2,1,0:T(8,128)(2,1)} %bitcast.48), calls=%async_computation | async-start | bytes 2097152 | tf_op jit(solution)/shard_map/all_to_all | solution.py:380
  170.3 5.1 %convolution_bitcast_fusion.1 = f32[1,2048,256]{2,1,0:T(8,128)} fusion(bf16[1024,2048]{1,0:T(8,128)(2,1)} %get-tuple-element.11, bf16[1024,256]{1,0:T(8,128)(2,1)} %copy-done.7), kind=kOutput, calls=%fused_computation.2 | convolution fusion | flops 1073741824 | bytes 6815744 | tf_op jit(solution)/shard_map/dot_general | solution.py:33
  175.4 0.0 copy-done.17
  175.4 0.0 copy-start.23
  175.5 2.7 %convolution_bitcast_fusion.2 = f32[1,2048,256]{2,1,0:T(8,128)} fusion(bf16[1024,2048]{1,0:T(8,128)(2,1)S(1)} %copy-done.17, bf16[1024,256]{1,0:T(8,128)(2,1)S(1)} %copy-done.6), kind=kOutput, calls=%fused_computation.3 | convolution fusion | flops 1073741824 | bytes 6815744 | tf_op jit(solution)/shard_map/dot_general | solution.py:33
  178.2 0.0 copy-done.15
  178.2 0.1 copy-done.21
  178.3 0.7 copy-done.23
  179.0 2.7 %convolution_bitcast_fusion = f32[1,256,2048]{2,1,0:T(8,128)} fusion(bf16[1024,2048]{1,0:T(8,128)(2,1)S(1)} %copy-done.15, f32[1024,256]{1,0:T(8,128)S(1)} %copy-done.23, f32[1024,256]{1,0:T(8,128)S(1)} %copy-done.21), kind=kOutput, calls=%fused_computation.1 | convolution fusion | flops 1075314688 | bytes 8388608 | tf_op jit(solution)/shard_map/dot_general | solution.py:33
  181.7 1.3 collective-permute-start.1
  182.9 0.7 constant_dynamic-slice_fusion
  183.7 3.5 %collective-permute-done.1 = f32[2,256]{1,0:T(2,128)S(1)} collective-permute-done((f32[2,256]{1,0:T(2,128)S(1)}, f32[2,256]{1,0:T(2,128)S(1)}, u32[]{:S(2)}, u32[]{:S(2)}) %collective-permute-start.1) | collective-permute-done | bytes 2080 | tf_op jit(solution)/shard_map/ppermute | solution.py:16
  187.1 0.8 fusion.30
  187.9 0.0 copy-done.9
  187.9 0.7 fusion.31
  188.6 8.0 %all-to-all-done = bf16[8,256,256]{2,1,0:T(8,128)(2,1)S(1)} async-done(((bf16[8,256,256]{2,1,0:T(8,128)(2,1)}), bf16[8,256,256]{2,1,0:T(8,128)(2,1)S(1)}, u32[]{:S(2)}, u32[]{:S(2)}) %all-to-all-start) | async-done | bytes 1048608 | tf_op jit(solution)/shard_map/all_to_all | solution.py:380
  196.6 0.8 convert_reduce_fusion
  (28 shorter events, 0.1 us)
Async XLA Ops:
  0.6 80.8 %copy-start = (bf16[1,2048,256]{2,1,0:T(8,128)(2,1)S(1)}, bf16[1,2048,256]{2,1,0:T(8,128)(2,1)}, u32[]{:S(2)}) copy-start(bf16[1,2048,256]{2,1,0:T(8,128)(2,1)} %param.21) | copy-start | bytes 3145732
  0.6 10.7 %copy-start.1 = (bf16[256,2048]{1,0:T(8,128)(2,1)S(1)}, bf16[256,2048]{1,0:T(8,128)(2,1)}, u32[]{:S(2)}) copy-start(bf16[256,2048]{1,0:T(8,128)(2,1)} %param.14) | copy-start | bytes 3145732
  1.8 159.4 %collective-permute-start = (f32[2,256]{1,0:T(2,128)S(1)}, f32[2,256]{1,0:T(2,128)S(1)}, u32[]{:S(2)}, u32[]{:S(2)}) collective-permute-start(f32[2,256]{1,0:T(2,128)S(1)} %slice.57), channel_id=1, source_target_pairs={{0,4},{4,8},{8,12},{12,16},{16,20},{20,24},{24,28},{1,5},{5,9},{9,... | collective-permute-start | bytes 6152 | tf_op jit(solution)/shard_map/ppermute | solution.py:16
  6.7 6.1 %copy-start.12 = (f32[2048]{0:T(1024)S(1)}, f32[2048]{0:T(1024)}, u32[]{:S(2)}) copy-start(f32[2048]{0:T(1024)} %param.15) | copy-start | bytes 24580
  81.4 3.6 %copy-start.3 = (bf16[1,2048,256]{2,1,0:T(8,128)(2,1)S(1)}, bf16[1,2048,256]{2,1,0:T(8,128)(2,1)}, u32[]{:S(2)}) copy-start(bf16[1,2048,256]{2,1,0:T(8,128)(2,1)} %param.22) | copy-start | bytes 3145732
  81.4 3.8 %copy-start.16 = (bf16[1024,2048]{1,0:T(8,128)(2,1)S(1)}, bf16[1024,2048]{1,0:T(8,128)(2,1)}, u32[]{:S(2)}) copy-start(bf16[1024,2048]{1,0:T(8,128)(2,1)} %get-tuple-element.11) | copy-start | bytes 12582916
  85.2 1.3 copy-start.20
  85.2 2.9 %copy-start.14 = (bf16[1024,2048]{1,0:T(8,128)(2,1)S(1)}, bf16[1024,2048]{1,0:T(8,128)(2,1)}, u32[]{:S(2)}) copy-start(bf16[1024,2048]{1,0:T(8,128)(2,1)} %get-tuple-element.10) | copy-start | bytes 12582916
  85.2 3.2 %copy-start.18 = (bf16[1,256,2048]{2,1,0:T(8,128)(2,1)S(1)}, bf16[1,256,2048]{2,1,0:T(8,128)(2,1)}, u32[]{:S(2)}) copy-start(bf16[1,256,2048]{2,1,0:T(8,128)(2,1)} %param.23) | copy-start | bytes 3145732
  86.5 3.6 %copy-start.22 = (f32[1024,256]{1,0:T(8,128)}, f32[1024,256]{1,0:T(8,128)S(1)}, u32[]{:S(2)}) copy-start(f32[1024,256]{1,0:T(8,128)S(1)} %fusion.6) | copy-start | bytes 3145732
  90.1 1.3 copy-start.5
  90.1 1.3 copy-start.7
  158.4 2.0 copy-start.2
  158.4 2.0 copy-start.4
  160.4 0.8 copy-start.13
  160.4 0.9 copy-start.11
  160.4 1.3 copy-start.19
  164.4 32.3 %all-to-all-start = ((bf16[8,256,256]{2,1,0:T(8,128)(2,1)}), bf16[8,256,256]{2,1,0:T(8,128)(2,1)S(1)}, u32[]{:S(2)}, u32[]{:S(2)}) async-start(bf16[8,256,256]{2,1,0:T(8,128)(2,1)} %bitcast.48), calls=%async_computation | async-start | bytes 2097152 | tf_op jit(solution)/shard_map/all_to_all | solution.py:380
  170.3 5.1 %copy-start.6 = (bf16[1024,256]{1,0:T(8,128)(2,1)S(1)}, bf16[1024,256]{1,0:T(8,128)(2,1)}, u32[]{:S(2)}) copy-start(bf16[1024,256]{1,0:T(8,128)(2,1)} %copy-done.5) | copy-start | bytes 1572868
  170.3 5.1 %copy-start.17 = (bf16[1024,2048]{1,0:T(8,128)(2,1)S(1)}, bf16[1024,2048]{1,0:T(8,128)(2,1)}, u32[]{:S(2)}) copy-start(bf16[1024,2048]{1,0:T(8,128)(2,1)} %get-tuple-element.11) | copy-start | bytes 12582916
  175.4 2.7 %copy-start.15 = (bf16[1024,2048]{1,0:T(8,128)(2,1)S(1)}, bf16[1024,2048]{1,0:T(8,128)(2,1)}, u32[]{:S(2)}) copy-start(bf16[1024,2048]{1,0:T(8,128)(2,1)} %get-tuple-element.10) | copy-start | bytes 12582916
  175.4 2.9 %copy-start.21 = (f32[1024,256]{1,0:T(8,128)S(1)}, f32[1024,256]{1,0:T(8,128)}, u32[]{:S(2)}) copy-start(f32[1024,256]{1,0:T(8,128)} %copy-done.20) | copy-start | bytes 3145732
  175.4 3.5 %copy-start.23 = (f32[1024,256]{1,0:T(8,128)S(1)}, f32[1024,256]{1,0:T(8,128)}, u32[]{:S(2)}) copy-start(f32[1024,256]{1,0:T(8,128)} %copy-done.22) | copy-start | bytes 3145732
  179.0 2.7 %copy-start.10 = (f32[256,256]{1,0:T(8,128)S(1)}, f32[256,256]{1,0:T(8,128)}, u32[]{:S(2)}) copy-start(f32[256,256]{1,0:T(8,128)} %get-tuple-element.18) | copy-start | bytes 786436
  179.0 8.2 %copy-start.8 = (bf16[256,256]{1,0:T(8,128)(2,1)S(1)}, bf16[256,256]{1,0:T(8,128)(2,1)}, u32[]{:S(2)}) copy-start(bf16[256,256]{1,0:T(8,128)(2,1)} %param.17) | copy-start | bytes 393220
  179.0 8.9 %copy-start.9 = (bf16[256,256]{1,0:T(8,128)(2,1)S(1)}, bf16[256,256]{1,0:T(8,128)(2,1)}, u32[]{:S(2)}) copy-start(bf16[256,256]{1,0:T(8,128)(2,1)} %param.18) | copy-start | bytes 393220
  181.7 5.5 %collective-permute-start.1 = (f32[2,256]{1,0:T(2,128)S(1)}, f32[2,256]{1,0:T(2,128)S(1)}, u32[]{:S(2)}, u32[]{:S(2)}) collective-permute-start(f32[2,256]{1,0:T(2,128)S(1)} %slice.60), channel_id=1, source_target_pairs={{4,0},{8,4},{12,8},{16,12},{20,16},{24,20},{28,24},{5,1},{9,5},{13... | collective-permute-start | bytes 6152 | tf_op jit(solution)/shard_map/ppermute | solution.py:16

commit v2 on v1

--- a/solution.py
+++ b/solution.py
@@ -59,6 +59,14 @@
     return pl.ds(pl.multiple_of(index * width, width), width)
 
 
+def mirrored(me, mask, n):
+    found, unit = 0, 1
+    while unit < n:
+        found = found + lax.rem(lax.div(me, unit) + lax.div(mask, unit), 2) * unit
+        unit = 2 * unit
+    return found
+
+
 def tp_places():
     tp, count = lax.axis_index("tp"), lax.axis_size("tp")
     cross = lax.rem(tp + count // 2, count)
@@ -97,10 +105,14 @@
         return outs[a].at[pl.ds(pl.multiple_of(block * depth, depth), depth), columns(column, width)]
 
     def source(k):
-        return lax.rem(me - k + n, n) if exchange else k
+        if not exchange:
+            return k
+        odd = k % 2
+        mask = odd * ((k + 1) // 2) + (1 - odd) * ((n - k // 2) % n)
+        return mirrored(me, jnp.int32(mask), n)
 
     def sent(a, k):
-        peer = lax.rem(me + k, n)
+        peer = source(k)
         return remote(
             ins[a].at[pl.ds(pl.multiple_of(peer * depth, depth), depth), :],
             block_of(a, me, tp),
@@ -207,7 +219,7 @@
     greet(True, cross, partner)
 
     def target(k):
-        return lax.rem(me + k + 1, n)
+        return mirrored(me, jnp.int32(n - 1 - k), n)
 
     def part(k, column):
         return partial[target(k), :, columns(column, width)].astype(jnp.float32)

time: 198 us -> 183 us (0.924)
  Pallas kernels: 128 us -> 115 us
  starting transfers between devices: 12.1 us -> 10.1 us
    pallas_call x1, Pallas kernels: 44.3 us -> 32.9 us  [returned_slots(): pl.pallas_call(functools.partial(return_kernel, n), out_shape=jax.ShapeDt...]
    all_to_all x1, starting transfers between devices: 5.96 us -> 3.95 us  [shards(): shares = lax.all_to_all(shares, 'sp', split_axis=0, concat_axis=0)]
  transfers between devices with their start and end apart: 3 -> 3, of which waited for: 2 -> 2; matrix products, arithmetic and copies ran while one was open for 19% -> 20% of each run, Pallas kernels for 65% -> 63%
where the time goes in v2:
time: 183 us
  Pallas kernels  115 us (63%)
  matrix products  28.3 us (15%)
  other arithmetic  11.6 us (6%)
  waiting for transfers between devices  11.5 us (6%)
  starting transfers between devices  10.1 us (6%)
  local copies, waits for them, and re-layouts  5.07 us (3%)
    pallas_call x2, Pallas kernels, gathered(): pl.pallas_call(functools.partial(gather_kernel, n, exchange, count), out_...  82.1 us
    pallas_call x1, Pallas kernels, returned_slots(): pl.pallas_call(functools.partial(return_kernel, n), out_shape=jax.ShapeDt...  32.9 us
    dot_general x5, matrix products, rows_product(): lax.dot_general(left, right, (((0,), (0,)), ((), ())), preferred_element_...  13.1 us
    all_to_all x1, waiting for transfers between devices, shards(): shares = lax.all_to_all(shares, 'sp', split_axis=0, concat_axis=0)  8.04 us
    ppermute x2, starting transfers between devices, passed_along(): lax.ppermute(value, axis, [(source, source + steps) for source in range(f...  6.18 us
    dot_general x3, matrix products, cols_product(): lax.dot_general(left, right, (((1,), (1,)), ((), ())), preferred_element_...  4.15 us
    all_to_all x1, starting transfers between devices, shards(): shares = lax.all_to_all(shares, 'sp', split_axis=0, concat_axis=0)  3.95 us
  transfers between devices with their start and end apart: 3, of which 2 were waited for; matrix products, arithmetic and copies ran while one was open for 20% of the time, Pallas kernels for 63%

profile of v2, /device:TPU:0, one launch (start us, length us, event | category | flops | bytes accessed | tf_op | source)
XLA Modules:
  0.0 182.6 jit_solution(4258085288601916786)
XLA Ops:
  0.6 0.0 copy-start
  0.6 0.0 copy-start.1
  0.7 1.1 convert_multiply_fusion.6
  1.8 4.9 %collective-permute-start = (f32[2,256]{1,0:T(2,128)S(1)}, f32[2,256]{1,0:T(2,128)S(1)}, u32[]{:S(2)}, u32[]{:S(2)}) collective-permute-start(f32[2,256]{1,0:T(2,128)S(1)} %slice.57), channel_id=1, source_target_pairs={{0,4},{4,8},{8,12},{12,16},{16,20},{20,24},{24,28},{1,5},{5,9},{9,... | collective-permute-start | bytes 6152 | tf_op jit(solution)/shard_map/ppermute | solution.py:16
  6.7 0.0 copy-start.12
  6.7 1.5 fusion
  8.3 0.7 fusion.40
  9.0 0.8 fusion.47
  9.7 0.2 convolution_convert_fusion.3
  9.9 0.7 select_reduce_fusion
  10.6 0.7 multiply_add_fusion
  11.3 0.0 copy-done.1
  11.3 1.5 convert_multiply_fusion
  12.8 0.0 copy-done.12
  12.8 0.1 dynamic-slice
  12.9 0.3 add_reduce_fusion
  13.2 2.4 %multiply_convert_fusion.refs_1_ = bf16[1024,512]{1,0:T(8,128)(2,1)} fusion(f32[1024]{0:T(1024)S(1)} %add_reduce_fusion, s32[256]{0:T(256)S(1)} %bitcast.60, s32[256]{0:T(256)S(1)} %bitcast.56, bf16[256,2048]{1,0:T(8,128)(2,1)} %param.13, s32[]{:T(128)S(6)} %select_n.17), kind=kOutput, calls=%fused_computation.12 | convolution fusion | flops 270270464 | bytes 1316868 | tf_op jit(solution)/shard_map/dot_general | solution.py:340
  15.6 2.5 %convolution_convert_fusion.1.refs_0_ = bf16[1024,512]{1,0:T(8,128)(2,1)} fusion(s32[256]{0:T(256)S(1)} %bitcast.61, s32[256]{0:T(256)S(1)} %bitcast.57, f32[256,2048]{1,0:T(8,128)} %convert_multiply_fusion, s32[]{:T(128)S(6)} %select_n.17, f32[512]{0:T(512)S(1)} %dynamic-slice), kind=kOutput, calls=%fused_computation.13 | convolution fusion | flops 270008320 | bytes 1576964 | tf_op jit(solution)/shard_map/dot_general | solution.py:342
  18.0 62.4 %shard_map.188 = (bf16[1024,2048]{1,0:T(8,128)(2,1)}, bf16[1024,2048]{1,0:T(8,128)(2,1)}) custom-call(bf16[1024,512]{1,0:T(8,128)(2,1)} %convolution_convert_fusion.1.refs_0_, bf16[1024,512]{1,0:T(8,128)(2,1)} %multiply_convert_fusion.refs_1_), custom_call_target="tpu_custom_call" | custom-call | tf_op jit(solution)/shard_map/pallas_call | solution.py:184
  80.4 0.0 copy-done
  80.4 0.0 copy-start.3
  80.4 3.6 %fusion.3 = f32[1024,256]{1,0:T(8,128)S(1)} fusion(bf16[1024,2048]{1,0:T(8,128)(2,1)} %get-tuple-element.11, bf16[1,2048,256]{2,1,0:T(8,128)(2,1)S(1)} %copy-done), kind=kOutput, calls=%fused_computation.18 | convolution fusion | flops 1073741824 | bytes 6291456 | tf_op jit(solution)/shard_map/dot_general | solution.py:349
  84.1 0.1 copy-done.16
  84.2 1.3 fusion.6
  85.5 0.0 copy-start.22
  85.5 1.7 copy-done.14
  87.1 0.3 copy-done.18
  87.4 1.6 multiply_convert_fusion.2
  89.0 0.0 copy-start.5
  89.1 1.3 fusion.1
  90.4 1.3 add_convert_fusion
  91.7 32.9 %shard_map.189 = bf16[8,128,512]{2,1,0:T(8,128)(2,1)S(1)} custom-call(bf16[8,128,2048]{2,1,0:T(8,128)(2,1)S(1)} %bitcast.46), custom_call_target="tpu_custom_call" | custom-call | tf_op jit(solution)/shard_map/pallas_call | solution.py:280
  124.6 1.2 convolution_convert_fusion.2.refs_0_
  125.8 19.8 %shard_map.190 = bf16[256,2048]{1,0:T(8,128)(2,1)} custom-call(bf16[256,512]{1,0:T(8,128)(2,1)} %convolution_convert_fusion.2.refs_0_), custom_call_target="tpu_custom_call" | custom-call | tf_op jit(solution)/shard_map/pallas_call | solution.py:184
  145.6 0.0 copy-start.2
  145.6 0.0 copy-start.4
  145.6 1.9 %multiply_reduce_fusion = f32[256]{0:T(256)S(1)} fusion(bf16[256,2048]{1,0:T(8,128)(2,1)} %shard_map.190, f32[2048]{0:T(1024)S(1)} %copy-done.12, f32[256]{0:T(256)S(1)} %add_rsqrt_fusion, bf16[256,2048]{1,0:T(8,128)(2,1)S(1)} %copy-done.1), kind=kLoop, calls=%fused_computation.10 | loop fusion | flops 3145472 | bytes 2107392 | tf_op jit(solution)/shard_map/reduce_sum | solution.py:373
  147.5 0.0 copy-done.2
  147.5 0.0 copy-done.4
  147.5 0.0 copy-start.13
  147.6 0.0 copy-start.11
  147.6 0.0 copy-start.19
  147.6 0.8 add_convert_fusion.1
  148.4 0.0 collective-permute-done
  148.4 0.0 copy-done.11
  148.5 0.4 copy-done.19
  148.9 1.2 multiply_convert_fusion.5
  150.1 1.5 convolution_convert_fusion
  151.5 3.9 %all-to-all-start = ((bf16[8,256,256]{2,1,0:T(8,128)(2,1)}), bf16[8,256,256]{2,1,0:T(8,128)(2,1)S(1)}, u32[]{:S(2)}, u32[]{:S(2)}) async-start(bf16[8,256,256]{2,1,0:T(8,128)(2,1)} %bitcast.48), calls=%async_computation | async-start | bytes 2097152 | tf_op jit(solution)/shard_map/all_to_all | solution.py:392
  155.5 0.0 copy-start.17
  155.5 5.1 %convolution_bitcast_fusion.1 = f32[1,2048,256]{2,1,0:T(8,128)} fusion(bf16[1024,2048]{1,0:T(8,128)(2,1)} %get-tuple-element.11, bf16[1024,256]{1,0:T(8,128)(2,1)} %copy-done.7), kind=kOutput, calls=%fused_computation.2 | convolution fusion | flops 1073741824 | bytes 6815744 | tf_op jit(solution)/shard_map/dot_general | solution.py:33
  160.6 0.0 copy-done.17
  160.6 0.0 copy-start.23
  160.6 2.7 %convolution_bitcast_fusion.2 = f32[1,2048,256]{2,1,0:T(8,128)} fusion(bf16[1024,2048]{1,0:T(8,128)(2,1)S(1)} %copy-done.17, bf16[1024,256]{1,0:T(8,128)(2,1)S(1)} %copy-done.6), kind=kOutput, calls=%fused_computation.3 | convolution fusion | flops 1073741824 | bytes 6815744 | tf_op jit(solution)/shard_map/dot_general | solution.py:33
  163.3 0.1 copy-done.21
  163.5 0.7 copy-done.23
  164.2 2.7 %convolution_bitcast_fusion = f32[1,256,2048]{2,1,0:T(8,128)} fusion(bf16[1024,2048]{1,0:T(8,128)(2,1)S(1)} %copy-done.15, f32[1024,256]{1,0:T(8,128)S(1)} %copy-done.23, f32[1024,256]{1,0:T(8,128)S(1)} %copy-done.21), kind=kOutput, calls=%fused_computation.1 | convolution fusion | flops 1075314688 | bytes 8388608 | tf_op jit(solution)/shard_map/dot_general | solution.py:33
  166.8 1.3 collective-permute-start.1
  168.1 0.7 constant_dynamic-slice_fusion
  168.8 3.5 %collective-permute-done.1 = f32[2,256]{1,0:T(2,128)S(1)} collective-permute-done((f32[2,256]{1,0:T(2,128)S(1)}, f32[2,256]{1,0:T(2,128)S(1)}, u32[]{:S(2)}, u32[]{:S(2)}) %collective-permute-start.1) | collective-permute-done | bytes 2080 | tf_op jit(solution)/shard_map/ppermute | solution.py:16
  172.3 0.8 fusion.30
  173.1 0.7 fusion.31
  173.7 8.0 %all-to-all-done = bf16[8,256,256]{2,1,0:T(8,128)(2,1)S(1)} async-done(((bf16[8,256,256]{2,1,0:T(8,128)(2,1)}), bf16[8,256,256]{2,1,0:T(8,128)(2,1)S(1)}, u32[]{:S(2)}, u32[]{:S(2)}) %all-to-all-start) | async-done | bytes 1048608 | tf_op jit(solution)/shard_map/all_to_all | solution.py:392
  181.8 0.8 convert_reduce_fusion
  (28 shorter events, 0.1 us)
Async XLA Ops:
  0.6 79.8 %copy-start = (bf16[1,2048,256]{2,1,0:T(8,128)(2,1)S(1)}, bf16[1,2048,256]{2,1,0:T(8,128)(2,1)}, u32[]{:S(2)}) copy-start(bf16[1,2048,256]{2,1,0:T(8,128)(2,1)} %param.21) | copy-start | bytes 3145732
  0.6 10.7 %copy-start.1 = (bf16[256,2048]{1,0:T(8,128)(2,1)S(1)}, bf16[256,2048]{1,0:T(8,128)(2,1)}, u32[]{:S(2)}) copy-start(bf16[256,2048]{1,0:T(8,128)(2,1)} %param.14) | copy-start | bytes 3145732
  1.8 146.6 %collective-permute-start = (f32[2,256]{1,0:T(2,128)S(1)}, f32[2,256]{1,0:T(2,128)S(1)}, u32[]{:S(2)}, u32[]{:S(2)}) collective-permute-start(f32[2,256]{1,0:T(2,128)S(1)} %slice.57), channel_id=1, source_target_pairs={{0,4},{4,8},{8,12},{12,16},{16,20},{20,24},{24,28},{1,5},{5,9},{9,... | collective-permute-start | bytes 6152 | tf_op jit(solution)/shard_map/ppermute | solution.py:16
  6.7 6.1 %copy-start.12 = (f32[2048]{0:T(1024)S(1)}, f32[2048]{0:T(1024)}, u32[]{:S(2)}) copy-start(f32[2048]{0:T(1024)} %param.15) | copy-start | bytes 24580
  80.4 3.6 %copy-start.3 = (bf16[1,2048,256]{2,1,0:T(8,128)(2,1)S(1)}, bf16[1,2048,256]{2,1,0:T(8,128)(2,1)}, u32[]{:S(2)}) copy-start(bf16[1,2048,256]{2,1,0:T(8,128)(2,1)} %param.22) | copy-start | bytes 3145732
  80.4 3.8 %copy-start.16 = (bf16[1024,2048]{1,0:T(8,128)(2,1)S(1)}, bf16[1024,2048]{1,0:T(8,128)(2,1)}, u32[]{:S(2)}) copy-start(bf16[1024,2048]{1,0:T(8,128)(2,1)} %get-tuple-element.11) | copy-start | bytes 12582916
  84.2 1.3 copy-start.20
  84.2 2.9 %copy-start.14 = (bf16[1024,2048]{1,0:T(8,128)(2,1)S(1)}, bf16[1024,2048]{1,0:T(8,128)(2,1)}, u32[]{:S(2)}) copy-start(bf16[1024,2048]{1,0:T(8,128)(2,1)} %get-tuple-element.10) | copy-start | bytes 12582916
  84.2 3.2 %copy-start.18 = (bf16[1,256,2048]{2,1,0:T(8,128)(2,1)S(1)}, bf16[1,256,2048]{2,1,0:T(8,128)(2,1)}, u32[]{:S(2)}) copy-start(bf16[1,256,2048]{2,1,0:T(8,128)(2,1)} %param.23) | copy-start | bytes 3145732
  85.5 3.6 %copy-start.22 = (f32[1024,256]{1,0:T(8,128)}, f32[1024,256]{1,0:T(8,128)S(1)}, u32[]{:S(2)}) copy-start(f32[1024,256]{1,0:T(8,128)S(1)} %fusion.6) | copy-start | bytes 3145732
  89.0 1.3 copy-start.5
  89.1 1.3 copy-start.7
  145.6 2.0 %copy-start.2 = (bf16[256,2048]{1,0:T(8,128)(2,1)S(1)}, bf16[256,2048]{1,0:T(8,128)(2,1)}, u32[]{:S(2)}) copy-start(bf16[256,2048]{1,0:T(8,128)(2,1)} %shard_map.190) | copy-start | bytes 3145732
  145.6 2.0 %copy-start.4 = (bf16[256,2048]{1,0:T(8,128)(2,1)S(1)}, bf16[256,2048]{1,0:T(8,128)(2,1)}, u32[]{:S(2)}) copy-start(bf16[256,2048]{1,0:T(8,128)(2,1)} %param.13) | copy-start | bytes 3145732
  147.5 0.8 copy-start.13
  147.6 0.9 copy-start.11
  147.6 1.3 copy-start.19
  151.5 30.3 %all-to-all-start = ((bf16[8,256,256]{2,1,0:T(8,128)(2,1)}), bf16[8,256,256]{2,1,0:T(8,128)(2,1)S(1)}, u32[]{:S(2)}, u32[]{:S(2)}) async-start(bf16[8,256,256]{2,1,0:T(8,128)(2,1)} %bitcast.48), calls=%async_computation | async-start | bytes 2097152 | tf_op jit(solution)/shard_map/all_to_all | solution.py:392
  155.5 5.1 %copy-start.6 = (bf16[1024,256]{1,0:T(8,128)(2,1)S(1)}, bf16[1024,256]{1,0:T(8,128)(2,1)}, u32[]{:S(2)}) copy-start(bf16[1024,256]{1,0:T(8,128)(2,1)} %copy-done.5) | copy-start | bytes 1572868
  155.5 5.1 %copy-start.17 = (bf16[1024,2048]{1,0:T(8,128)(2,1)S(1)}, bf16[1024,2048]{1,0:T(8,128)(2,1)}, u32[]{:S(2)}) copy-start(bf16[1024,2048]{1,0:T(8,128)(2,1)} %get-tuple-element.11) | copy-start | bytes 12582916
  160.6 2.7 %copy-start.15 = (bf16[1024,2048]{1,0:T(8,128)(2,1)S(1)}, bf16[1024,2048]{1,0:T(8,128)(2,1)}, u32[]{:S(2)}) copy-start(bf16[1024,2048]{1,0:T(8,128)(2,1)} %get-tuple-element.10) | copy-start | bytes 12582916
  160.6 2.9 %copy-start.21 = (f32[1024,256]{1,0:T(8,128)S(1)}, f32[1024,256]{1,0:T(8,128)}, u32[]{:S(2)}) copy-start(f32[1024,256]{1,0:T(8,128)} %copy-done.20) | copy-start | bytes 3145732
  160.6 3.5 %copy-start.23 = (f32[1024,256]{1,0:T(8,128)S(1)}, f32[1024,256]{1,0:T(8,128)}, u32[]{:S(2)}) copy-start(f32[1024,256]{1,0:T(8,128)} %copy-done.22) | copy-start | bytes 3145732
  164.1 2.7 %copy-start.10 = (f32[256,256]{1,0:T(8,128)S(1)}, f32[256,256]{1,0:T(8,128)}, u32[]{:S(2)}) copy-start(f32[256,256]{1,0:T(8,128)} %get-tuple-element.18) | copy-start | bytes 786436
  164.1 8.1 %copy-start.8 = (bf16[256,256]{1,0:T(8,128)(2,1)S(1)}, bf16[256,256]{1,0:T(8,128)(2,1)}, u32[]{:S(2)}) copy-start(bf16[256,256]{1,0:T(8,128)(2,1)} %param.17) | copy-start | bytes 393220
  164.1 8.9 %copy-start.9 = (bf16[256,256]{1,0:T(8,128)(2,1)S(1)}, bf16[256,256]{1,0:T(8,128)(2,1)}, u32[]{:S(2)}) copy-start(bf16[256,256]{1,0:T(8,128)(2,1)} %param.18) | copy-start | bytes 393220
  166.8 5.5 %collective-permute-start.1 = (f32[2,256]{1,0:T(2,128)S(1)}, f32[2,256]{1,0:T(2,128)S(1)}, u32[]{:S(2)}, u32[]{:S(2)}) collective-permute-start(f32[2,256]{1,0:T(2,128)S(1)} %slice.60), channel_id=1, source_target_pairs={{4,0},{8,4},{12,8},{16,12},{20,16},{24,20},{28,24},{5,1},{9,5},{13... | collective-permute-start | bytes 6152 | tf_op jit(solution)/shard_map/ppermute | solution.py:16
